TPU v7x, 32 devices: a whole 2x2x4 slice. The times are simulated.
32 devices in a mesh: ep: 16 (over z, y, x), tp: 2 (over core).
Axes of the slice: x: 2, y: 2, z: 4, core: 2. Of those that a mesh axis runs over, the one named last changes fastest.
Arguments:
- tokens: bfloat16 [384, 2048], P('ep'), may hold values from -6 to 6
- attn_gain: float32 [2048], replicated, may hold values from 0.1 to 1.9
- w_query: bfloat16 [2048, 1024], P(None, 'tp'), may hold values from -0.125 to 0.125
- w_key: bfloat16 [2048, 1024], P(None, 'tp'), may hold values from -0.125 to 0.125
- w_value: bfloat16 [2048, 1024], P(None, 'tp'), may hold values from -0.125 to 0.125
- w_zgate: bfloat16 [2048, 1024], P(None, 'tp'), may hold values from -0.125 to 0.125
- w_decay: bfloat16 [2048, 8], P(None, 'tp'), may hold values from -0.125 to 0.125
- w_beta: bfloat16 [2048, 8], P(None, 'tp'), may hold values from -0.125 to 0.125
- decay_rate: float32 [8], P('tp'), may hold values from 0.05 to 2
- decay_bias: float32 [8], P('tp'), may hold values from -3 to 3
- state: float32 [384, 8, 128, 128], P('ep', 'tp'), may hold values from -2 to 2
- out_gain: float32 [128], replicated, may hold values from 0.1 to 1.9
- w_out: bfloat16 [1024, 2048], P('tp'), may hold values from -0.1875 to 0.1875
- ffn_gain: float32 [2048], replicated, may hold values from 0.1 to 1.9
- expert_gate: bfloat16 [16, 2048, 512], P('ep', None, 'tp'), may hold values from -0.125 to 0.125
- expert_up: bfloat16 [16, 2048, 512], P('ep', None, 'tp'), may hold values from -0.125 to 0.125
- expert_down: bfloat16 [16, 512, 2048], P('ep', 'tp'), may hold values from -0.25 to 0.25
- routes: int32 [384, 2], P('ep'), may hold values from 0 to 15, all different within a row; in each aligned block of 24 rows (0 to 23, 24 to 47, ...) at most 6 rows name the same one
- route_weight: float32 [384, 2], P('ep'), may hold values from 0.2 to 1
Outputs:
- layer_out: bfloat16 [384, 2048], P('ep', 'tp')
- new_state: float32 [384, 8, 128, 128], P('ep', 'tp')
Inputs may be any that keep to these rules, and one draw needn't show every extreme that they name: `routes`: the 2 entries of a row differ. Among the rows of one index of ep (aligned blocks of 24 rows) no expert is named more than 6 times, a bound that some block reaches.
All inputs are finite; a program needn't handle non-finite values.
Results may differ from a plain program's by a relative error of at most 0.014.
Values may be sent and summed in bfloat16 or wider, within the bound.
A program may use at most 128 MiB of HBM per device.

v0:
```python
import jax
import jax.numpy as jnp
from jax import lax
from jax.sharding import PartitionSpec as P

EPS = 1e-06


def rms_scale(rows, gain):
    return rows * lax.rsqrt(jnp.mean(rows * rows, axis=-1, keepdims=True) + EPS) * gain


def unit_rows(rows):
    return rows * lax.rsqrt(jnp.sum(rows * rows, axis=-1, keepdims=True) + EPS)


def per_device(
    tokens,
    attn_gain,
    w_query,
    w_key,
    w_value,
    w_zgate,
    w_decay,
    w_beta,
    decay_rate,
    decay_bias,
    state,
    out_gain,
    w_out,
    ffn_gain,
    expert_gate,
    expert_up,
    expert_down,
    routes,
    route_weight,
):
    seqs, width = tokens.shape
    heads = state.shape[1]
    head_dim = state.shape[2]
    top = routes.shape[1]
    resid_in = tokens.astype(jnp.float32)
    normed = rms_scale(resid_in, attn_gain).astype(jnp.bfloat16)

    def project(weight):
        return jnp.dot(normed, weight, preferred_element_type=jnp.float32).astype(jnp.bfloat16)

    def heads_of(raw):
        return raw.reshape(seqs, heads, head_dim).astype(jnp.float32)

    query = unit_rows(jax.nn.silu(heads_of(project(w_query)))) * head_dim ** (-0.5)
    key = unit_rows(jax.nn.silu(heads_of(project(w_key))))
    value = jax.nn.silu(heads_of(project(w_value)))
    zmul = jax.nn.silu(heads_of(project(w_zgate)))
    fade = jnp.exp(-decay_rate * jax.nn.softplus(project(w_decay).astype(jnp.float32) + decay_bias))
    beta = jax.nn.sigmoid(project(w_beta).astype(jnp.float32))
    predicted = jnp.einsum("shkv,shk->shv", state, key, precision=lax.Precision.HIGHEST)
    written = beta[..., None] * (value - fade[..., None] * predicted)
    new_state = fade[..., None, None] * state + key[..., :, None] * written[..., None, :]
    read = jnp.einsum("shkv,shk->shv", new_state, query, precision=lax.Precision.HIGHEST)
    heads_out = (
        (rms_scale(read, out_gain) * zmul).astype(jnp.bfloat16).reshape(seqs, heads * head_dim)
    )
    partial_value = jnp.dot(heads_out, w_out, preferred_element_type=jnp.float32)
    mixed = lax.psum(partial_value.astype(jnp.bfloat16), "tp").astype(jnp.float32)
    resid = resid_in + mixed
    moe_in = rms_scale(resid, ffn_gain).astype(jnp.bfloat16)
    experts = lax.axis_size("ep")
    cap = max(2, 2 * seqs * top // experts)
    flat_routes = routes.reshape(-1)
    onehot = (flat_routes[:, None] == jnp.arange(experts, dtype=jnp.int32)[None, :]).astype(
        jnp.int32
    )
    before = jnp.cumsum(onehot, axis=0) - onehot
    slot = jnp.sum(before * onehot, axis=1)
    place = flat_routes * cap + slot
    pick = (place[:, None] == jnp.arange(experts * cap, dtype=jnp.int32)[None, :]).astype(
        jnp.bfloat16
    )
    columns = width // lax.axis_size("tp")
    own_part = lax.dynamic_slice_in_dim(moe_in, lax.axis_index("tp") * columns, columns, 1)
    spread = jnp.repeat(own_part, top, axis=0)
    outgoing = jnp.dot(pick.T, spread, preferred_element_type=jnp.float32).astype(jnp.bfloat16)
    outgoing = outgoing.reshape(experts, 1, cap, columns)
    arrived = lax.all_gather(
        lax.all_to_all(outgoing, "ep", split_axis=0, concat_axis=1, tiled=True),
        "tp",
        axis=3,
        tiled=True,
    )
    flat_rows = arrived.reshape(-1, arrived.shape[-1])
    gate = jnp.dot(flat_rows, expert_gate[0], preferred_element_type=jnp.float32)
    up = jnp.dot(flat_rows, expert_up[0], preferred_element_type=jnp.float32)
    hidden = (jax.nn.silu(gate) * up).astype(jnp.bfloat16)
    term = jnp.dot(hidden, expert_down[0], preferred_element_type=jnp.float32)
    terms = term.reshape(arrived.shape[:-1] + (term.shape[-1],))
    summed = lax.psum_scatter(terms.astype(jnp.bfloat16), "tp", scatter_dimension=3, tiled=True)
    returned = lax.all_to_all(summed, "ep", split_axis=1, concat_axis=0, tiled=True)
    returned = returned.reshape(experts * cap, columns)
    per_route = jnp.dot(pick, returned, preferred_element_type=jnp.float32).reshape(
        seqs, top, columns
    )
    combined = jnp.sum(per_route * route_weight[..., None], axis=1)
    own_resid = lax.dynamic_slice_in_dim(resid, lax.axis_index("tp") * columns, columns, 1)
    layer_out = (own_resid + combined).astype(jnp.bfloat16)
    return (layer_out, new_state)


def solution(mesh):
    in_specs = (
        P("ep", None),
        P(),
        P(None, "tp"),
        P(None, "tp"),
        P(None, "tp"),
        P(None, "tp"),
        P(None, "tp"),
        P(None, "tp"),
        P("tp"),
        P("tp"),
        P("ep", "tp", None, None),
        P(),
        P("tp", None),
        P(),
        P("ep", None, "tp"),
        P("ep", None, "tp"),
        P("ep", "tp", None),
        P("ep", None),
        P("ep", None),
    )
    out_specs = (P("ep", "tp"), P("ep", "tp", None, None))
    return jax.shard_map(
        per_device, mesh=mesh, in_specs=in_specs, out_specs=out_specs, check_vma=False
    )
```

profile of v0, /device:TPU:0, one launch (start us, length us, event | category | flops | bytes accessed | tf_op | source)
XLA Modules:
  0.0 115.3 jit_solution(10898759450930380615)
XLA Ops:
  7.2 0.0 copy-start
  7.2 0.0 copy-start.2
  7.2 0.0 copy-start.5
  7.2 0.0 copy-start.12
  7.2 0.0 all-reduce.2.cloned.1.call-start
  7.3 1.2 %fusion.18 = f32[24]{0:T(128)S(1)} fusion(bf16[24,2048]{1,0:T(8,128)(2,1)} %param.19), kind=kLoop, calls=%fused_computation.33 | loop fusion | flops 147432 | bytes 98400 | tf_op jit(solution)/shard_map/reduce_sum | solution.py:10
  8.4 0.0 copy-start.11
  8.5 2.1 %fusion.6 = f32[24,512]{1,0:T(8,128)S(1)} fusion(bf16[2048,512]{1,0:T(8,128)(2,1)} %param.22, bf16[24,2048]{1,0:T(8,128)(2,1)} %param.19, f32[2048]{0:T(1024)} %param.20, f32[24]{0:T(128)S(1)} %add_rsqrt_fusion.4), kind=kOutput, calls=%fused_computation.16 | convolution fusion | flops 50552832 | bytes 2252896 | tf_op jit(solution)/shard_map/dot_general | solution.py:46
  10.6 0.1 multiply_reduce_fusion.3
  10.7 0.1 broadcast_multiply_fusion
  10.8 0.0 copy-done.12
  10.9 0.2 fusion.34
  11.1 0.1 copy.48
  11.2 2.0 %fusion.5 = f32[24,512]{1,0:T(8,128)S(1)} fusion(bf16[2048,512]{1,0:T(8,128)(2,1)} %param.23, bf16[24,2048]{1,0:T(8,128)(2,1)S(1)} %copy-done.2, f32[2048]{0:T(1024)S(1)} %copy-done.5, f32[24]{0:T(128)S(1)} %add_rsqrt_fusion.4), kind=kOutput, calls=%fused_computation.14 | convolution fusion | flops 50552832 | bytes 2252896 | tf_op jit(solution)/shard_map/dot_general | solution.py:46
  13.3 0.2 fusion.13
  13.5 0.1 copy.49
  13.6 8.1 %fusion.41 = f32[24,4,1,128]{3,2,1,0:T(1,128)S(1)} fusion(f32[24,4,128,1]{2,3,1,0:T(1,128)S(1)} %bitcast.48, f32[24,4,128,128]{3,2,1,0:T(8,128)} %param.29), kind=kOutput, calls=%fused_computation.73 | convolution fusion | flops 18874368 | bytes 6389760 | tf_op jit(solution)/shard_map/shkv,shk->shv/dot_general | solution.py:57
  21.7 0.1 fusion.24
  21.8 0.0 copy-start.3
  21.8 3.9 %multiply_add_fusion = f32[24,4,128,128]{3,2,1,0:T(8,128)} fusion(f32[24,4,128,128]{3,2,1,0:T(8,128)S(1)} %copy-done.1, f32[24,4,128]{2,1,0:T(4,128)S(1)} %fusion.24, f32[24,4,128]{2,1,0:T(4,128)S(1)} %broadcast_multiply_fusion, f32[24,4]{1,0:T(8,128)S(1)} %copy.48), kind=kLoop, calls=%fused_computation | loop fusion | flops 4718592 | bytes 12681600 | tf_op jit(solution)/shard_map/add | solution.py:59
  25.7 0.4 fusion.4
  26.2 0.1 multiply_reduce_fusion.2
  26.3 0.1 multiply_multiply_fusion
  26.4 0.0 copy-start.4
  26.4 7.5 %fusion.42 = f32[24,4,1,128]{3,2,1,0:T(1,128)S(1)} fusion(f32[24,4,128,128]{3,2,1,0:T(8,128)} %multiply_add_fusion, f32[24,4,128,1]{2,3,1,0:T(1,128)S(1)} %bitcast.51), kind=kOutput, calls=%fused_computation.74 | convolution fusion | flops 18874368 | bytes 6389760 | tf_op jit(solution)/shard_map/shkv,shk->shv/dot_general | solution.py:60
  33.9 0.1 multiply_reduce_fusion.1
  34.1 0.0 copy-start.6
  34.1 0.0 copy-start.7
  34.1 0.4 fusion.3
  34.6 0.0 copy-done.9
  34.6 0.1 fusion.25
  34.7 1.0 convolution_convert_fusion.1
  35.7 0.0 all-reduce.2.cloned.1.call-update
  35.8 0.0 reduce-scatter.2.cloned.1.call-start
  35.8 0.1 copy.51
  35.9 0.1 eq.50
  36.0 0.1 fusion.28
  36.1 0.1 reduce_window_sum.11
  36.2 0.2 select_reduce_fusion
  36.4 0.0 copy-done.7
  36.4 20.1 %all-reduce.2.cloned.1.call-done = bf16[24,2048]{1,0:T(8,128)(2,1)} async-done(((bf16[24,2048]{1,0:T(8,128)(2,1)}), bf16[24,2048]{1,0:T(8,128)(2,1)}) %all-reduce.2.cloned.1.call-update) | async-done | bytes 98320 | tf_op jit(solution)/shard_map/psum | solution.py:65
  56.5 1.0 multiply_reduce_fusion
  57.5 0.1 multiply_convert_fusion
  57.6 0.1 broadcast_in_dim.2
  57.7 0.3 convolution_convert_fusion.2
  58.0 0.1 reshape.136
  58.1 16.9 %all_to_all.21 = bf16[16,1,6,1024]{3,2,1,0:T(8,128)(2,1)S(1)} all-to-all(bf16[16,1,6,1024]{3,2,1,0:T(8,128)(2,1)S(1)} %bitcast.47), channel_id=1, replica_groups=mesh['ep'=16,'tp'=2] {'ep'}, dimensions={0} | all-to-all | bytes 393216 | tf_op jit(solution)/shard_map/all_to_all | solution.py:86
  75.0 2.2 %all-gather = bf16[16,1,6,2048]{3,2,1,0:T(8,128)(2,1)S(1)} all-gather(bf16[16,1,6,1024]{3,2,1,0:T(8,128)(2,1)S(1)} %all_to_all.21), channel_id=2, replica_groups=mesh['ep'=16,'tp'=2] {'tp'}, dimensions={3}, use_global_device_ids=true | all-gather | bytes 589824 | tf_op jit(solution)/shard_map/all_gather | solution.py:85
  77.2 0.1 reshape.137
  77.3 1.5 %fusion.16 = f32[96,256]{1,0:T(8,128)S(1)} fusion(bf16[96,2048]{1,0:T(8,128)(2,1)S(1)} %reshape.137, bf16[1,2048,256]{2,1,0:T(8,128)(2,1)} %param.33), kind=kOutput, calls=%fused_computation.28 | convolution fusion | flops 100663296 | bytes 1540096 | tf_op jit(solution)/shard_map/dot_general | solution.py:92
  78.9 1.5 %fusion.2 = bf16[96,256]{1,0:T(8,128)(2,1)S(1)} fusion(bf16[96,2048]{1,0:T(8,128)(2,1)S(1)} %reshape.137, bf16[1,2048,256]{2,1,0:T(8,128)(2,1)} %param.34, f32[96,256]{1,0:T(8,128)S(1)} %fusion.16), kind=kOutput, calls=%fused_computation.8 | convolution fusion | flops 100810752 | bytes 1589248 | tf_op jit(solution)/shard_map/dot_general | solution.py:93
  80.4 0.0 copy-start.8
  80.5 2.3 %fusion = bf16[1,16,6,2048]{3,1,2,0:T(8,128)(2,1)} fusion(bf16[1,256,2048]{2,1,0:T(8,128)(2,1)} %param.35, bf16[16,6,256]{2,1,0:T(8,128)(2,1)S(1)} %dot_general.56), kind=kOutput, calls=%fused_computation.2 | convolution fusion | flops 100859904 | bytes 1490944 | tf_op jit(solution)/shard_map/dot_general | solution.py:95
  82.7 0.0 reduce-scatter.2.cloned.1.call-update
  82.8 5.9 %reduce-scatter.2.cloned.1.call-done = bf16[1,16,6,1024]{3,1,2,0:T(8,128)(2,1)} async-done(((bf16[1,16,6,2048]{3,1,2,0:T(8,128)(2,1)}), bf16[1,16,6,1024]{3,1,2,0:T(8,128)(2,1)}) %reduce-scatter.2.cloned.1.call-update) | async-done | bytes 196624 | tf_op jit(solution)/shard_map/reduce_scatter | solution.py:97
  88.6 1.7 %copy.55 = bf16[1,16,6,1024]{3,2,0,1:T(8,128)(2,1)} copy(bf16[1,16,6,1024]{3,1,2,0:T(8,128)(2,1)} %reduce-scatter.2.cloned.1.call-done) | data formatting | bytes 393216 | tf_op jit(solution)/shard_map/reduce_scatter | solution.py:97
  90.4 6.7 %all-to-all-start.1 = ((bf16[1,16,6,1024]{3,2,0,1:T(8,128)(2,1)}), bf16[1,16,6,1024]{3,2,0,1:T(8,128)(2,1)S(1)}, u32[]{:S(2)}, u32[]{:S(2)}) async-start(bf16[1,16,6,1024]{3,2,0,1:T(8,128)(2,1)} %copy.55), calls=%async_computation.2 | async-start | bytes 524288 | tf_op jit(solution)/shard_map/all_to_all | solution.py:98
  97.1 0.1 reduce_sum.70
  97.2 0.1 copy.52
  97.3 10.2 %all-to-all-done.1 = bf16[1,16,6,1024]{3,2,0,1:T(8,128)(2,1)S(1)} async-done(((bf16[1,16,6,1024]{3,2,0,1:T(8,128)(2,1)}), bf16[1,16,6,1024]{3,2,0,1:T(8,128)(2,1)S(1)}, u32[]{:S(2)}, u32[]{:S(2)}) %all-to-all-start.1) | async-done | bytes 196640 | tf_op jit(solution)/shard_map/all_to_all | solution.py:98
  107.5 0.1 reshape.150
  107.6 0.0 copy-done.8
  107.6 0.2 fusion.1
  107.8 0.6 add_convert_fusion
  (29 shorter events, 0.2 us)
Async XLA Ops:
  7.2 27.5 %copy-start = (bf16[512,2048]{1,0:T(8,128)(2,1)S(1)}, bf16[512,2048]{1,0:T(8,128)(2,1)}, u32[]{:S(2)}) copy-start(bf16[512,2048]{1,0:T(8,128)(2,1)} %param.31) | copy-start | bytes 6291460
  7.2 3.7 %copy-start.2 = (bf16[24,2048]{1,0:T(8,128)(2,1)S(1)}, bf16[24,2048]{1,0:T(8,128)(2,1)}, u32[]{:S(2)}) copy-start(bf16[24,2048]{1,0:T(8,128)(2,1)} %param.19) | copy-start | bytes 294916
  7.2 3.7 %copy-start.5 = (f32[2048]{0:T(1024)S(1)}, f32[2048]{0:T(1024)}, u32[]{:S(2)}) copy-start(f32[2048]{0:T(1024)} %param.20) | copy-start | bytes 24580
  7.2 3.6 %copy-start.12 = (f32[4]{0:T(128)S(1)}, f32[4]{0:T(128)}, u32[]{:S(2)}) copy-start(f32[4]{0:T(128)} %param.27) | copy-start | bytes 52
  7.2 3.7 %copy-start.10 = (bf16[2048,4]{0,1:T(4,128)(2,1)S(1)}, bf16[2048,4]{0,1:T(4,128)(2,1)}, u32[]{:S(2)}) copy-start(bf16[2048,4]{0,1:T(4,128)(2,1)} %param.25) | copy-start | bytes 49156
  7.2 3.7 %copy-start.13 = (f32[4]{0:T(128)S(1)}, f32[4]{0:T(128)}, u32[]{:S(2)}) copy-start(f32[4]{0:T(128)} %param.28) | copy-start | bytes 52
  7.2 49.2 %all-reduce.2.cloned.1.call-start = ((), (), s32[]{:S(2)}) async-start(), calls=%async_computation.3 | async-start | bytes 196608 | tf_op jit(solution)/shard_map/psum | solution.py:65
  8.4 4.8 %copy-start.11 = (bf16[2048,4]{0,1:T(4,128)(2,1)S(1)}, bf16[2048,4]{0,1:T(4,128)(2,1)}, u32[]{:S(2)}) copy-start(bf16[2048,4]{0,1:T(4,128)(2,1)} %param.26) | copy-start | bytes 49156
  13.6 8.2 %copy-start.1 = (f32[24,4,128,128]{3,2,1,0:T(8,128)S(1)}, f32[24,4,128,128]{3,2,1,0:T(8,128)}, u32[]{:S(2)}) copy-start(f32[24,4,128,128]{3,2,1,0:T(8,128)} %param.29) | copy-start | bytes 18874372
  21.8 3.9 %copy-start.3 = (bf16[2048,512]{1,0:T(8,128)(2,1)S(1)}, bf16[2048,512]{1,0:T(8,128)(2,1)}, u32[]{:S(2)}) copy-start(bf16[2048,512]{1,0:T(8,128)(2,1)} %param.21) | copy-start | bytes 6291460
  26.4 7.7 %copy-start.4 = (bf16[2048,512]{1,0:T(8,128)(2,1)S(1)}, bf16[2048,512]{1,0:T(8,128)(2,1)}, u32[]{:S(2)}) copy-start(bf16[2048,512]{1,0:T(8,128)(2,1)} %param.24) | copy-start | bytes 6291460
  33.9 0.7 copy-start.9
  34.1 1.7 %copy-start.6 = (s32[24,2]{0,1:T(2,128)S(1)}, s32[24,2]{0,1:T(2,128)}, u32[]{:S(2)}) copy-start(s32[24,2]{0,1:T(2,128)} %param.36) | copy-start | bytes 580
  34.1 2.3 %copy-start.7 = (f32[2048]{0:T(1024)S(1)}, f32[2048]{0:T(1024)}, u32[]{:S(2)}) copy-start(f32[2048]{0:T(1024)} %param.32) | copy-start | bytes 24580
  35.8 52.9 %reduce-scatter.2.cloned.1.call-start = ((), (), s32[]{:S(2)}) async-start(), calls=%async_computation.4 | async-start | bytes 589824 | tf_op jit(solution)/shard_map/reduce_scatter | solution.py:97
  80.4 27.2 %copy-start.8 = (f32[24,2]{0,1:T(2,128)S(1)}, f32[24,2]{0,1:T(2,128)}, u32[]{:S(2)}) copy-start(f32[24,2]{0,1:T(2,128)} %param.37) | copy-start | bytes 580
  90.4 17.1 %all-to-all-start.1 = ((bf16[1,16,6,1024]{3,2,0,1:T(8,128)(2,1)}), bf16[1,16,6,1024]{3,2,0,1:T(8,128)(2,1)S(1)}, u32[]{:S(2)}, u32[]{:S(2)}) async-start(bf16[1,16,6,1024]{3,2,0,1:T(8,128)(2,1)} %copy.55), calls=%async_computation.2 | async-start | bytes 524288 | tf_op jit(solution)/shard_map/all_to_all | solution.py:98
Sparse Core Ops, SparseCore 0:
  35.9 20.5 all-reduce.1
  82.9 5.7 reduce-scatter.1
where the time goes:
time: 116 us; the launch traced here: 115 us
  waiting for transfers between devices  36.2 us (31%)
  matrix products  28 us (24%)
  blocking collectives  19.1 us (16%)
  between operations  14.4 us (12%)
  other arithmetic  7.91 us (7%)
  starting transfers between devices  6.81 us (6%)
  local copies, waits for them, and re-layouts  2.86 us (2%)
    psum x1, waiting for transfers between devices, per_device(): lax.psum(partial_value.astype(jnp.bfloat16), 'tp').astype(jnp.float32)  20.1 us
    all_to_all x1, blocking collectives, per_device(): lax.all_to_all(outgoing, 'ep', split_axis=0, concat_axis=1, tiled=True)  16.9 us
    all_to_all x1, waiting for transfers between devices, per_device(): lax.all_to_all(summed, 'ep', split_axis=1, concat_axis=0, tiled=True)  10.2 us
    dot_general x1, matrix products, per_device(): jnp.einsum('shkv,shk->shv', state, key, precision=lax.Precision.HIGHEST)  8.09 us
    dot_general x1, matrix products, per_device(): jnp.einsum('shkv,shk->shv', new_state, query, precision=lax.Precision.HIG...  7.54 us
    all_to_all x1, starting transfers between devices, per_device(): lax.all_to_all(summed, 'ep', split_axis=1, concat_axis=0, tiled=True)  6.73 us
    reduce_scatter x1, waiting for transfers between devices, per_device(): lax.psum_scatter(terms.astype(jnp.bfloat16), 'tp', scatter_dimension=3, t...  5.89 us
    dot_general x6, matrix products, project(): jnp.dot(normed, weight, preferred_element_type=jnp.float32)  5.45 us
  transfers between devices with their start and end apart: 3, of which 3 were waited for; matrix products, arithmetic and copies ran while one was open for 1% of the time, Pallas kernels for 0%

commit v1 on v0

--- a/solution.py
+++ b/solution.py
@@ -95,7 +95,10 @@
     term = jnp.dot(hidden, expert_down[0], preferred_element_type=jnp.float32)
     terms = term.reshape(arrived.shape[:-1] + (term.shape[-1],))
     summed = lax.psum_scatter(terms.astype(jnp.bfloat16), "tp", scatter_dimension=3, tiled=True)
-    returned = lax.all_to_all(summed, "ep", split_axis=1, concat_axis=0, tiled=True)
+    returned = jnp.concatenate(
+        lax.all_to_all(jnp.stack(jnp.split(summed, lax.psum(1, "ep"), axis=1), axis=0), "ep", 0, 0),
+        axis=0,
+    )
     returned = returned.reshape(experts * cap, columns)
     per_route = jnp.dot(pick, returned, preferred_element_type=jnp.float32).reshape(
         seqs, top, columns

time: 116 us -> 126 us (1.086)
  local copies, waits for them, and re-layouts: 2.86 us -> 13.1 us
    unnamed x29 -> x44, local copies, waits for them, and re-layouts: 0.2 us -> 9.3 us
    split x0 -> x1, local copies, waits for them, and re-layouts: none -> 2.23 us  [per_device(): jnp.split(summed, lax.psum(1, 'ep'), axis=1)]
    reduce_scatter x1 -> x0, local copies, waits for them, and re-layouts: 1.73 us -> none  [per_device(): lax.psum_scatter(terms.astype(jnp.bfloat16), 'tp', scatter_dimension=3, t...]
where the time goes in v1:
time: 126 us
  waiting for transfers between devices  36.2 us (29%)
  matrix products  28 us (22%)
  blocking collectives  19.1 us (15%)
  between operations  14.5 us (12%)
  local copies, waits for them, and re-layouts  13.1 us (10%)
  other arithmetic  7.91 us (6%)
  starting transfers between devices  6.81 us (5%)
    psum x1, waiting for transfers between devices, per_device(): lax.psum(partial_value.astype(jnp.bfloat16), 'tp').astype(jnp.float32)  20.1 us
    all_to_all x1, blocking collectives, per_device(): lax.all_to_all(outgoing, 'ep', split_axis=0, concat_axis=1, tiled=True)  16.9 us
    all_to_all x1, waiting for transfers between devices, per_device(): lax.all_to_all(jnp.stack(jnp.split(summed, lax.psum(1, 'ep'), axis=1), ax...  10.2 us
    unnamed x44, local copies, waits for them, and re-layouts  9.3 us
    dot_general x1, matrix products, per_device(): jnp.einsum('shkv,shk->shv', state, key, precision=lax.Precision.HIGHEST)  8.09 us
    dot_general x1, matrix products, per_device(): jnp.einsum('shkv,shk->shv', new_state, query, precision=lax.Precision.HIG...  7.54 us
    all_to_all x1, starting transfers between devices, per_device(): lax.all_to_all(jnp.stack(jnp.split(summed, lax.psum(1, 'ep'), axis=1), ax...  6.73 us
    reduce_scatter x1, waiting for transfers between devices, per_device(): lax.psum_scatter(terms.astype(jnp.bfloat16), 'tp', scatter_dimension=3, t...  5.89 us
  transfers between devices with their start and end apart: 3, of which 3 were waited for; matrix products, arithmetic and copies ran while one was open for 1% of the time, Pallas kernels for 0%

profile of v1, /device:TPU:0, one launch (start us, length us, event | category | flops | bytes accessed | tf_op | source)
XLA Modules:
  0.0 125.5 jit_solution(14143242713647247710)
XLA Ops:
  7.3 1.2 fusion.18
  8.5 2.1 %fusion.6 = f32[24,512]{1,0:T(8,128)S(1)} fusion(bf16[2048,512]{1,0:T(8,128)(2,1)} %param.22, bf16[24,2048]{1,0:T(8,128)(2,1)} %param.19, f32[2048]{0:T(1024)} %param.20, f32[24]{0:T(128)S(1)} %add_rsqrt_fusion.4), kind=kOutput, calls=%fused_computation.16 | convolution fusion | flops 50552832 | bytes 2252896 | tf_op jit(solution)/shard_map/dot_general | solution.py:46
  10.6 0.1 multiply_reduce_fusion.3
  10.7 0.1 broadcast_multiply_fusion
  10.9 0.2 fusion.34
  11.1 0.1 copy.286
  11.2 2.0 %fusion.5 = f32[24,512]{1,0:T(8,128)S(1)} fusion(bf16[2048,512]{1,0:T(8,128)(2,1)} %param.23, bf16[24,2048]{1,0:T(8,128)(2,1)S(1)} %copy-done.2, f32[2048]{0:T(1024)S(1)} %copy-done.5, f32[24]{0:T(128)S(1)} %add_rsqrt_fusion.4), kind=kOutput, calls=%fused_computation.14 | convolution fusion | flops 50552832 | bytes 2252896 | tf_op jit(solution)/shard_map/dot_general | solution.py:46
  13.3 0.2 fusion.13
  13.5 0.1 copy.287
  13.6 8.1 %fusion.42 = f32[24,4,1,128]{3,2,1,0:T(1,128)S(1)} fusion(f32[24,4,128,1]{2,3,1,0:T(1,128)S(1)} %bitcast.78, f32[24,4,128,128]{3,2,1,0:T(8,128)} %param.29), kind=kOutput, calls=%fused_computation.90 | convolution fusion | flops 18874368 | bytes 6389760 | tf_op jit(solution)/shard_map/shkv,shk->shv/dot_general | solution.py:57
  21.7 0.1 fusion.24
  21.8 3.9 %multiply_add_fusion = f32[24,4,128,128]{3,2,1,0:T(8,128)} fusion(f32[24,4,128,128]{3,2,1,0:T(8,128)S(1)} %copy-done.1, f32[24,4,128]{2,1,0:T(4,128)S(1)} %fusion.24, f32[24,4,128]{2,1,0:T(4,128)S(1)} %broadcast_multiply_fusion, f32[24,4]{1,0:T(8,128)S(1)} %copy.286), kind=kLoop, calls=%fused_computation | loop fusion | flops 4718592 | bytes 12681600 | tf_op jit(solution)/shard_map/add | solution.py:59
  25.7 0.4 fusion.4
  26.2 0.1 multiply_reduce_fusion.2
  26.3 0.1 multiply_multiply_fusion
  26.4 7.5 %fusion.43 = f32[24,4,1,128]{3,2,1,0:T(1,128)S(1)} fusion(f32[24,4,128,128]{3,2,1,0:T(8,128)} %multiply_add_fusion, f32[24,4,128,1]{2,3,1,0:T(1,128)S(1)} %bitcast.81), kind=kOutput, calls=%fused_computation.91 | convolution fusion | flops 18874368 | bytes 6389760 | tf_op jit(solution)/shard_map/shkv,shk->shv/dot_general | solution.py:60
  33.9 0.1 multiply_reduce_fusion.1
  34.1 0.4 fusion.3
  34.6 0.0 copy-done.9
  34.6 0.1 fusion.25
  34.7 1.0 convolution_convert_fusion.1
  35.8 0.0 reduce-scatter.2.cloned.1.call-start
  35.8 0.1 copy.289
  35.9 0.1 eq.50
  36.0 0.1 fusion.28
  36.1 0.1 reduce_window_sum.11
  36.2 0.2 select_reduce_fusion
  36.4 20.1 %all-reduce.2.cloned.1.call-done = bf16[24,2048]{1,0:T(8,128)(2,1)} async-done(((bf16[24,2048]{1,0:T(8,128)(2,1)}), bf16[24,2048]{1,0:T(8,128)(2,1)}) %all-reduce.2.cloned.1.call-update) | async-done | bytes 98320 | tf_op jit(solution)/shard_map/psum | solution.py:65
  56.5 1.0 multiply_reduce_fusion
  57.5 0.1 multiply_convert_fusion
  57.6 0.1 broadcast_in_dim.2
  57.7 0.3 convolution_convert_fusion.2
  58.0 0.1 reshape.129
  58.1 16.9 %all_to_all.17 = bf16[16,1,6,1024]{3,2,1,0:T(8,128)(2,1)S(1)} all-to-all(bf16[16,1,6,1024]{3,2,1,0:T(8,128)(2,1)S(1)} %bitcast.77), channel_id=1, replica_groups=mesh['ep'=16,'tp'=2] {'ep'}, dimensions={0} | all-to-all | bytes 393216 | tf_op jit(solution)/shard_map/all_to_all | solution.py:86
  75.0 2.2 %all-gather = bf16[16,1,6,2048]{3,2,1,0:T(8,128)(2,1)S(1)} all-gather(bf16[16,1,6,1024]{3,2,1,0:T(8,128)(2,1)S(1)} %all_to_all.17), channel_id=2, replica_groups=mesh['ep'=16,'tp'=2] {'tp'}, dimensions={3}, use_global_device_ids=true | all-gather | bytes 589824 | tf_op jit(solution)/shard_map/all_gather | solution.py:85
  77.2 0.1 reshape.130
  77.3 1.5 %fusion.16 = f32[96,256]{1,0:T(8,128)S(1)} fusion(bf16[96,2048]{1,0:T(8,128)(2,1)S(1)} %reshape.130, bf16[1,2048,256]{2,1,0:T(8,128)(2,1)} %param.33), kind=kOutput, calls=%fused_computation.28 | convolution fusion | flops 100663296 | bytes 1540096 | tf_op jit(solution)/shard_map/dot_general | solution.py:92
  78.9 1.5 %fusion.2 = bf16[96,256]{1,0:T(8,128)(2,1)S(1)} fusion(bf16[96,2048]{1,0:T(8,128)(2,1)S(1)} %reshape.130, bf16[1,2048,256]{2,1,0:T(8,128)(2,1)} %param.34, f32[96,256]{1,0:T(8,128)S(1)} %fusion.16), kind=kOutput, calls=%fused_computation.8 | convolution fusion | flops 100810752 | bytes 1589248 | tf_op jit(solution)/shard_map/dot_general | solution.py:93
  80.5 2.3 %fusion = bf16[1,16,6,2048]{3,1,2,0:T(8,128)(2,1)} fusion(bf16[1,256,2048]{2,1,0:T(8,128)(2,1)} %param.35, bf16[16,6,256]{2,1,0:T(8,128)(2,1)S(1)} %dot_general.56), kind=kOutput, calls=%fused_computation.2 | convolution fusion | flops 100859904 | bytes 1490944 | tf_op jit(solution)/shard_map/dot_general | solution.py:95
  82.8 5.9 %reduce-scatter.2.cloned.1.call-done = bf16[1,16,6,1024]{3,1,2,0:T(8,128)(2,1)} async-done(((bf16[1,16,6,2048]{3,1,2,0:T(8,128)(2,1)}), bf16[1,16,6,1024]{3,1,2,0:T(8,128)(2,1)}) %reduce-scatter.2.cloned.1.call-update) | async-done | bytes 196624 | tf_op jit(solution)/shard_map/reduce_scatter | solution.py:97
  88.7 2.2 %fusion.41 = (bf16[1,1,6,1024]{3,1,2,0:T(2,128)(2,1)S(1)}, bf16[1,1,6,1024]{3,1,2,0:T(2,128)(2,1)S(1)}, bf16[1,1,6,1024]{3,1,2,0:T(2,128)(2,1)S(1)}, bf16[1,1,6,...) fusion(bf16[1,16,6,1024]{3,1,2,0:T(8,128)(2,1)} %reduce-scatter, ...), kind=kLoop, calls=%fused_computation.89 | loop fusion | bytes 393216 | tf_op jit(solution)/shard_map/split | solution.py:99
  90.9 0.6 constant_dynamic-update-slice_fusion.15
  91.5 0.6 constant_dynamic-update-slice_fusion.14
  92.1 0.6 constant_dynamic-update-slice_fusion.13
  92.7 0.6 constant_dynamic-update-slice_fusion.12
  93.3 0.6 constant_dynamic-update-slice_fusion.11
  93.9 0.6 constant_dynamic-update-slice_fusion.10
  94.5 0.6 constant_dynamic-update-slice_fusion.9
  95.1 0.6 constant_dynamic-update-slice_fusion.8
  95.7 0.6 constant_dynamic-update-slice_fusion.7
  96.3 0.6 constant_dynamic-update-slice_fusion.6
  97.0 0.6 constant_dynamic-update-slice_fusion.5
  97.6 0.6 constant_dynamic-update-slice_fusion.4
  98.2 0.6 constant_dynamic-update-slice_fusion.3
  98.8 0.6 constant_dynamic-update-slice_fusion.2
  99.4 0.6 constant_dynamic-update-slice_fusion.1
  100.0 0.6 constant_dynamic-update-slice_fusion
  100.6 6.7 %all-to-all-start.1 = ((bf16[16,1,1,6,1024]{4,3,2,1,0:T(8,128)(2,1)}), bf16[16,1,1,6,1024]{4,3,2,1,0:T(8,128)(2,1)S(1)}, u32[]{:S(2)}, u32[]{:S(2)}) async-start(bf16[16,1,1,6,1024]{4,3,2,1,0:T(8,128)(2,1)} %constant_dynamic-update-slice_fusion), calls=%async_computation.2 | async-start | bytes 524288 | tf_op jit(solution)/shard_map/all_to_all | solution.py:99
  107.3 0.1 reduce_sum.70
  107.4 0.1 copy.290
  107.5 10.2 %all-to-all-done.1 = bf16[16,1,1,6,1024]{4,3,2,1,0:T(8,128)(2,1)S(1)} async-done(((bf16[16,1,1,6,1024]{4,3,2,1,0:T(8,128)(2,1)}), bf16[16,1,1,6,1024]{4,3,2,1,0:T(8,128)(2,1)S(1)}, u32[]{:S(2)}, u32[]{:S(2)}) %all-to-all-start.1) | async-done | bytes 196640 | tf_op jit(solution)/shard_map/all_to_all | solution.py:99
  117.7 0.1 reshape.142
  117.8 0.2 fusion.1
  118.0 0.6 add_convert_fusion
  (45 shorter events, 0.4 us)
Async XLA Ops:
  7.2 27.5 %copy-start = (bf16[512,2048]{1,0:T(8,128)(2,1)S(1)}, bf16[512,2048]{1,0:T(8,128)(2,1)}, u32[]{:S(2)}) copy-start(bf16[512,2048]{1,0:T(8,128)(2,1)} %param.31) | copy-start | bytes 6291460
  7.2 3.7 %copy-start.2 = (bf16[24,2048]{1,0:T(8,128)(2,1)S(1)}, bf16[24,2048]{1,0:T(8,128)(2,1)}, u32[]{:S(2)}) copy-start(bf16[24,2048]{1,0:T(8,128)(2,1)} %param.19) | copy-start | bytes 294916
  7.2 3.7 %copy-start.5 = (f32[2048]{0:T(1024)S(1)}, f32[2048]{0:T(1024)}, u32[]{:S(2)}) copy-start(f32[2048]{0:T(1024)} %param.20) | copy-start | bytes 24580
  7.2 3.6 %copy-start.12 = (f32[4]{0:T(128)S(1)}, f32[4]{0:T(128)}, u32[]{:S(2)}) copy-start(f32[4]{0:T(128)} %param.27) | copy-start | bytes 52
  7.2 3.7 %copy-start.10 = (bf16[2048,4]{0,1:T(4,128)(2,1)S(1)}, bf16[2048,4]{0,1:T(4,128)(2,1)}, u32[]{:S(2)}) copy-start(bf16[2048,4]{0,1:T(4,128)(2,1)} %param.25) | copy-start | bytes 49156
  7.2 3.7 %copy-start.13 = (f32[4]{0:T(128)S(1)}, f32[4]{0:T(128)}, u32[]{:S(2)}) copy-start(f32[4]{0:T(128)} %param.28) | copy-start | bytes 52
  7.2 49.2 %all-reduce.2.cloned.1.call-start = ((), (), s32[]{:S(2)}) async-start(), calls=%async_computation.3 | async-start | bytes 196608 | tf_op jit(solution)/shard_map/psum | solution.py:65
  8.4 4.8 %copy-start.11 = (bf16[2048,4]{0,1:T(4,128)(2,1)S(1)}, bf16[2048,4]{0,1:T(4,128)(2,1)}, u32[]{:S(2)}) copy-start(bf16[2048,4]{0,1:T(4,128)(2,1)} %param.26) | copy-start | bytes 49156
  13.6 8.2 %copy-start.1 = (f32[24,4,128,128]{3,2,1,0:T(8,128)S(1)}, f32[24,4,128,128]{3,2,1,0:T(8,128)}, u32[]{:S(2)}) copy-start(f32[24,4,128,128]{3,2,1,0:T(8,128)} %param.29) | copy-start | bytes 18874372
  21.8 3.9 %copy-start.3 = (bf16[2048,512]{1,0:T(8,128)(2,1)S(1)}, bf16[2048,512]{1,0:T(8,128)(2,1)}, u32[]{:S(2)}) copy-start(bf16[2048,512]{1,0:T(8,128)(2,1)} %param.21) | copy-start | bytes 6291460
  26.4 7.7 %copy-start.4 = (bf16[2048,512]{1,0:T(8,128)(2,1)S(1)}, bf16[2048,512]{1,0:T(8,128)(2,1)}, u32[]{:S(2)}) copy-start(bf16[2048,512]{1,0:T(8,128)(2,1)} %param.24) | copy-start | bytes 6291460
  33.9 0.7 copy-start.9
  34.1 1.7 %copy-start.6 = (s32[24,2]{0,1:T(2,128)S(1)}, s32[24,2]{0,1:T(2,128)}, u32[]{:S(2)}) copy-start(s32[24,2]{0,1:T(2,128)} %param.36) | copy-start | bytes 580
  34.1 2.3 %copy-start.7 = (f32[2048]{0:T(1024)S(1)}, f32[2048]{0:T(1024)}, u32[]{:S(2)}) copy-start(f32[2048]{0:T(1024)} %param.32) | copy-start | bytes 24580
  35.8 52.9 %reduce-scatter.2.cloned.1.call-start = ((), (), s32[]{:S(2)}) async-start(), calls=%async_computation.4 | async-start | bytes 589824 | tf_op jit(solution)/shard_map/reduce_scatter | solution.py:97
  80.4 37.4 %copy-start.8 = (f32[24,2]{0,1:T(2,128)S(1)}, f32[24,2]{0,1:T(2,128)}, u32[]{:S(2)}) copy-start(f32[24,2]{0,1:T(2,128)} %param.37) | copy-start | bytes 580
  100.6 17.1 %all-to-all-start.1 = ((bf16[16,1,1,6,1024]{4,3,2,1,0:T(8,128)(2,1)}), bf16[16,1,1,6,1024]{4,3,2,1,0:T(8,128)(2,1)S(1)}, u32[]{:S(2)}, u32[]{:S(2)}) async-start(bf16[16,1,1,6,1024]{4,3,2,1,0:T(8,128)(2,1)} %constant_dynamic-update-slice_fusion), calls=%async_computation.2 | async-start | bytes 524288 | tf_op jit(solution)/shard_map/all_to_all | solution.py:99
Sparse Core Ops, SparseCore 0:
  35.9 20.5 all-reduce.1
  82.9 5.7 reduce-scatter.1
